TPU v7x, 32 devices: a whole 2x2x4 slice. The times are simulated.
32 devices in a mesh: ep: 16 (over z, y, x), tp: 2 (over core).
Axes of the slice: x: 2, y: 2, z: 4, core: 2. Of those that a mesh axis runs over, the one named last changes fastest.
Arguments:
- tokens: bfloat16 [512, 2048], P('ep'), may hold values from -6 to 6
- mix_gain: float32 [2048], replicated, may hold values from 0.1 to 1.9
- w_query: bfloat16 [2048, 512], P('ep', 'tp'), may hold values from -0.125 to 0.125
- w_key: bfloat16 [2048, 512], P('ep', 'tp'), may hold values from -0.125 to 0.125
- w_value: bfloat16 [2048, 512], P('ep', 'tp'), may hold values from -0.125 to 0.125
- w_outgate: bfloat16 [2048, 512], P('ep', 'tp'), may hold values from -0.125 to 0.125
- w_igate: bfloat16 [2048, 8], P('ep', 'tp'), may hold values from -0.125 to 0.125
- w_fgate: bfloat16 [2048, 8], P('ep', 'tp'), may hold values from -0.125 to 0.125
- igate_bias: float32 [8], P('tp'), may hold values from -2 to 1
- fgate_bias: float32 [8], P('tp'), may hold values from 0 to 4
- head_gain: float32 [512], P('tp'), may hold values from 0.1 to 1.9
- w_out: bfloat16 [512, 2048], P('tp', 'ep'), may hold values from -0.25 to 0.25
- state_matrix: float32 [512, 8, 64, 64], P('ep', 'tp'), may hold values from -2.4 to 2.4
- state_norm: float32 [512, 8, 64], P('ep', 'tp'), may hold values from -2.4 to 2.4
- state_max: float32 [512, 8], P('ep', 'tp'), may hold values from -4 to 4
- ffn_gain: float32 [2048], replicated, may hold values from 0.1 to 1.9
- w_expert_gate: bfloat16 [16, 2048, 1408], P('ep', None, 'tp'), may hold values from -0.125 to 0.125
- w_expert_up: bfloat16 [16, 2048, 1408], P('ep', None, 'tp'), may hold values from -0.125 to 0.125
- w_expert_down: bfloat16 [16, 1408, 2048], P('ep', 'tp'), may hold values from -0.15625 to 0.15625
- routes: int32 [512, 3], P('ep'), may hold values from 0 to 15, all different within a row; in each aligned block of 32 rows (0 to 31, 32 to 63, ...) at most 12 rows name the same one
- route_weights: float32 [512, 3], P('ep'), may hold values from 0.2 to 1
Outputs:
- mixed: bfloat16 [512, 2048], P('ep')
- new_matrix: float32 [512, 8, 64, 64], P('ep', 'tp')
- new_norm: float32 [512, 8, 64], P('ep', 'tp')
- new_max: float32 [512, 8], P('ep', 'tp')
Inputs may be any that keep to these rules, and one draw needn't show every extreme that they name: `routes`: each row names 3 different experts. Among the rows of one device, no expert is named by more than 12 rows, a bound that some block reaches.
All inputs are finite; a program needn't handle non-finite values.
Results may differ from a plain program's by a relative error of at most 0.017.
Values may be sent and summed in bfloat16 or wider, within the bound.
No kernel may reach another device: no remote copies, remote signals or barrier semaphores. Data moves between devices by JAX's collectives and lax.ppermute only.
A program may use at most 128 MiB of HBM per device.

v0:
```python
import jax
import jax.numpy as jnp
from jax import lax
from jax.sharding import PartitionSpec as P


def rms_scale(values_in, gain_vec):
    widened = values_in.astype(jnp.float32)
    return (
        widened * lax.rsqrt(jnp.mean(widened * widened, axis=-1, keepdims=True) + 1e-06) * gain_vec
    )


def memory_cell(
    query,
    key_row,
    value_row,
    outgate,
    input_pre,
    forget_pre,
    head_gain,
    state_matrix,
    state_norm,
    state_max,
):
    seq_rows, head_count = input_pre.shape
    head_size = query.shape[1] // head_count
    query_heads = query.astype(jnp.float32).reshape(seq_rows, head_count, head_size)
    key_heads = key_row.astype(jnp.float32).reshape(
        seq_rows, head_count, head_size
    ) * head_size ** (-0.5)
    value_heads = value_row.astype(jnp.float32).reshape(seq_rows, head_count, head_size)
    log_forget = jax.nn.log_sigmoid(forget_pre)
    new_max = jnp.maximum(log_forget + state_max, input_pre)
    keep_old = jnp.exp(log_forget + state_max - new_max)
    keep_new = jnp.exp(input_pre - new_max)
    new_matrix = (
        keep_old[:, :, None, None] * state_matrix
        + keep_new[:, :, None, None] * value_heads[:, :, :, None] * key_heads[:, :, None, :]
    )
    new_norm = keep_old[:, :, None] * state_norm + keep_new[:, :, None] * key_heads
    numerator = jnp.einsum(
        "bhvd,bhd->bhv", new_matrix, query_heads, precision=lax.Precision.HIGHEST
    )
    denominator = jnp.sum(new_norm * query_heads, axis=-1)
    cell_read = numerator / jnp.maximum(jnp.abs(denominator), jnp.exp(-new_max))[:, :, None]
    centered = cell_read - jnp.mean(cell_read, axis=-1, keepdims=True)
    variance = jnp.mean(centered * centered, axis=-1, keepdims=True)
    scaled_cell = (centered * lax.rsqrt(variance + 1e-06)).reshape(seq_rows, head_count * head_size)
    cell_out = (scaled_cell * head_gain * jax.nn.sigmoid(outgate.astype(jnp.float32))).astype(
        jnp.bfloat16
    )
    return (cell_out, new_matrix, new_norm, new_max)


def body(
    tokens,
    mix_gain,
    w_query,
    w_key,
    w_value,
    w_outgate,
    w_igate,
    w_fgate,
    igate_bias,
    fgate_bias,
    head_gain,
    w_out,
    state_matrix,
    state_norm,
    state_max,
    ffn_gain,
    w_expert_gate,
    w_expert_up,
    w_expert_down,
    routes,
    route_weights,
):
    seq_rows, width = tokens.shape
    normed = rms_scale(tokens, mix_gain).astype(jnp.bfloat16)
    weight_list = (w_query, w_key, w_value, w_outgate, w_igate, w_fgate)
    spread = lax.all_to_all(normed, "ep", split_axis=1, concat_axis=0, tiled=True)
    joined = jnp.concatenate(weight_list, axis=1)
    summed = lax.psum_scatter(
        jnp.dot(spread, joined, preferred_element_type=jnp.float32),
        "ep",
        scatter_dimension=0,
        tiled=True,
    )
    bounds = [0]
    for weight in weight_list:
        bounds.append(bounds[-1] + weight.shape[1])
    projected = tuple(
        (summed[:, bounds[index] : bounds[index + 1]] for index in range(len(weight_list)))
    )
    query = projected[0].astype(jnp.bfloat16)
    key_row = projected[1].astype(jnp.bfloat16)
    value_row = projected[2].astype(jnp.bfloat16)
    outgate = projected[3].astype(jnp.bfloat16)
    input_pre = projected[4] + igate_bias
    forget_pre = projected[5] + fgate_bias
    cell_out, new_matrix, new_norm, new_max = memory_cell(
        query,
        key_row,
        value_row,
        outgate,
        input_pre,
        forget_pre,
        head_gain,
        state_matrix,
        state_norm,
        state_max,
    )
    partial_out = jnp.dot(
        cell_out,
        lax.all_gather(w_out, "ep", axis=1, tiled=True),
        preferred_element_type=jnp.float32,
    )
    attended = lax.psum(partial_out.astype(jnp.bfloat16), "tp").astype(jnp.float32)
    resid = (tokens.astype(jnp.float32) + attended).astype(jnp.bfloat16)
    normed_two = rms_scale(resid, ffn_gain).astype(jnp.bfloat16)
    ep_count = lax.axis_size("ep")
    local_experts = w_expert_gate.shape[0]
    expert_total = local_experts * ep_count
    top_count = routes.shape[1]
    capacity = max(2, 2 * seq_rows * top_count // expert_total)
    flat_routes = routes.reshape(-1)
    onehot = (flat_routes[:, None] == jnp.arange(expert_total, dtype=jnp.int32)[None, :]).astype(
        jnp.int32
    )
    earlier = jnp.cumsum(onehot, axis=0, dtype=jnp.int32) - onehot
    slots = jnp.sum(onehot * earlier, axis=1, dtype=jnp.int32)
    targets = flat_routes * capacity + slots
    dispatch = (
        targets[:, None] == jnp.arange(expert_total * capacity, dtype=jnp.int32)[None, :]
    ).astype(jnp.bfloat16)
    route_rows = jnp.repeat(normed_two, top_count, axis=0)
    outgoing = jnp.einsum(
        "rs,rd->sd", dispatch, route_rows, preferred_element_type=jnp.float32
    ).astype(jnp.bfloat16)
    outgoing = outgoing.reshape(expert_total, capacity, width)
    received = lax.all_to_all(outgoing, "ep", split_axis=0, concat_axis=0, tiled=True)
    slot_count = received.shape[1]
    regrouped = received.reshape(ep_count, local_experts, slot_count, width)
    gate_pre = jnp.einsum(
        "nxcd,xdf->nxcf", regrouped, w_expert_gate, preferred_element_type=jnp.float32
    )
    up_pre = jnp.einsum(
        "nxcd,xdf->nxcf", regrouped, w_expert_up, preferred_element_type=jnp.float32
    )
    hidden = (jax.nn.silu(gate_pre) * up_pre).astype(jnp.bfloat16)
    partial_down = jnp.einsum(
        "nxcf,xfd->nxcd", hidden, w_expert_down, preferred_element_type=jnp.float32
    )
    expert_sum = lax.psum(partial_down.astype(jnp.bfloat16), "tp")
    finished = expert_sum.reshape(ep_count * local_experts, slot_count, width)
    returned = lax.all_to_all(finished, "ep", split_axis=0, concat_axis=0, tiled=True)
    picked = jnp.dot(
        dispatch,
        returned.reshape(expert_total * capacity, width),
        preferred_element_type=jnp.float32,
    )
    weighted = jnp.sum(
        picked.reshape(seq_rows, top_count, width) * route_weights[:, :, None], axis=1
    )
    mixed = (resid.astype(jnp.float32) + weighted).astype(jnp.bfloat16)
    return (mixed, new_matrix, new_norm, new_max)


def solution(mesh):
    placed = (
        P("ep", None),
        P(),
        P("ep", "tp"),
        P("ep", "tp"),
        P("ep", "tp"),
        P("ep", "tp"),
        P("ep", "tp"),
        P("ep", "tp"),
        P("tp"),
        P("tp"),
        P("tp"),
        P("tp", "ep"),
        P("ep", "tp", None, None),
        P("ep", "tp", None),
        P("ep", "tp"),
        P(),
        P("ep", None, "tp"),
        P("ep", None, "tp"),
        P("ep", "tp", None),
        P("ep", None),
        P("ep", None),
    )
    return jax.shard_map(
        body,
        mesh=mesh,
        in_specs=placed,
        out_specs=(P("ep", None), P("ep", "tp", None, None), P("ep", "tp", None), P("ep", "tp")),
        check_vma=False,
    )
```

profile of v0, /device:TPU:8, one launch (start us, length us, event | category | flops | bytes accessed | tf_op | source)
XLA Modules:
  0.0 342.0 jit_solution(8380659892496630698)
XLA Ops:
  7.2 1.2 fusion.36
  8.4 1.7 copy_bitcast_fusion
  10.1 7.2 %all-to-all-start = ((bf16[32,16,128]{2,0,1:T(8,128)(2,1)}), bf16[32,16,128]{2,0,1:T(8,128)(2,1)S(1)}, u32[]{:S(2)}, u32[]{:S(2)}) async-start(bf16[32,16,128]{2,0,1:T(8,128)(2,1)} %copy_bitcast_fusion), calls=%async_computation | async-start | bytes 262144 | tf_op jit(solution)/shard_map/all_to_all | solution.py:82
  17.3 0.8 copy.58
  18.1 0.8 copy.59
  19.0 1.1 concatenate.3
  20.0 3.9 %all-to-all-done = bf16[32,16,128]{2,0,1:T(8,128)(2,1)S(1)} async-done(((bf16[32,16,128]{2,0,1:T(8,128)(2,1)}), bf16[32,16,128]{2,0,1:T(8,128)(2,1)S(1)}, u32[]{:S(2)}, u32[]{:S(2)}) %all-to-all-start) | async-done | bytes 131104 | tf_op jit(solution)/shard_map/all_to_all | solution.py:82
  23.9 1.9 fusion.62
  25.8 0.7 all-gather.2.cloned.1.call-update
  26.8 0.1 eq.50
  27.0 0.1 reduce_window_sum.11
  27.1 0.2 select_reduce_fusion
  27.3 125.7 %reduce-scatter.2.cloned.1.call-done = f32[32,1032]{1,0:T(8,128)} async-done(((f32[512,1032]{1,0:T(8,128)}), f32[32,1032]{1,0:T(8,128)}) %reduce-scatter.2.cloned.1.call-update) | async-done | bytes 132112 | tf_op jit(solution)/shard_map/reduce_scatter | solution.py:84
  153.0 0.9 convert.9
  154.1 0.1 reshape.171
  154.4 0.9 broadcast_multiply_fusion.3
  155.3 0.8 subtract_exponential_fusion.1
  156.1 0.8 multiply_reduce_fusion.1
  156.9 3.8 %multiply_add_fusion = f32[32,4,64,64]{3,2,1,0:T(8,128)S(1)} fusion(f32[32,4,64,64]{3,2,1,0:T(8,128)} %param.33, f32[32,4,64]{2,1,0:T(4,128)S(1)} %get-tuple-element.30, f32[32,4,64]{2,1,0:T(4,128)S(1)} %get-tuple-element.31, f32[32,4]{1,0:T(8,128)S(1)} %subtract_exponential_fusion.1), kind=kLoop, calls=%fused_computation | loop fusion | flops 1572864 | bytes 4260352 | tf_op jit(solution)/shard_map/add | solution.py:38
  160.7 2.0 copy-done.1
  162.7 3.4 fusion.63
  166.1 0.2 fusion.59
  166.3 0.2 multiply_reduce_fusion
  166.5 0.1 subtract_multiply_fusion
  166.6 0.1 reshape.152
  166.7 39.0 %all-gather.2.cloned.1.call-done = bf16[256,2048]{1,0:T(8,128)(2,1)} async-done(((bf16[256,128]{1,0:T(8,128)(2,1)}), bf16[256,2048]{1,0:T(8,128)(2,1)}) %all-gather.2.cloned.1.call-update) | async-done | bytes 1048592 | tf_op jit(solution)/shard_map/all_gather | solution.py:116
  205.7 2.2 convolution_convert_fusion.1
  207.9 0.5 multiply_add_fusion.3
  208.4 18.1 %all-reduce.3.cloned.1.call-done = bf16[32,2048]{1,0:T(8,128)(2,1)} async-done(((bf16[32,2048]{1,0:T(8,128)(2,1)}), bf16[32,2048]{1,0:T(8,128)(2,1)}) %all-reduce.3.cloned.1.call-update) | async-done | bytes 131088 | tf_op jit(solution)/shard_map/psum | solution.py:119
  226.5 1.1 fusion.40
  227.6 1.0 fusion.42
  228.6 0.2 broadcast_in_dim.2
  228.8 1.1 reshape.153
  229.9 2.4 convolution_convert_fusion
  232.3 2.1 reshape.154
  234.4 33.1 %all_to_all.29 = bf16[16,12,2048]{2,1,0:T(8,128)(2,1)S(1)} all-to-all(bf16[16,12,2048]{2,1,0:T(8,128)(2,1)} %reshape.154), channel_id=1, replica_groups=mesh['ep'=16,'tp'=2] {'ep'}, dimensions={0} | all-to-all | bytes 1572864 | tf_op jit(solution)/shard_map/all_to_all | solution.py:142
  267.5 1.0 copy-done.4
  268.5 3.8 %fusion.9 = f32[16,1,12,704]{3,0,2,1:T(8,128)} fusion(bf16[1,2048,704]{1,2,0:T(8,128)(2,1)} %param.37, bf16[16,12,2048]{2,1,0:T(8,128)(2,1)S(1)} %all_to_all.29), kind=kOutput, calls=%fused_computation.11 | convolution fusion | flops 553648128 | bytes 4210688 | tf_op jit(solution)/shard_map/nxcd,xdf->nxcf/dot_general | solution.py:145
  272.3 5.2 %fusion.6 = bf16[16,12,2048]{2,0,1:T(8,128)(2,1)} fusion(bf16[1,704,2048]{2,1,0:T(8,128)(2,1)S(1)} %copy-done, bf16[1,2048,704]{1,2,0:T(8,128)(2,1)} %param.38, f32[16,1,12,704]{3,0,2,1:T(8,128)} %fusion.9, bf16[16,12,2048]{2,1,0:T(8,128)(2,1)} %copy-done.4), kind=kOutput, calls=%fused_computation.7 | convolution fusion | flops 1108500480 | bytes 7880704 | tf_op jit(solution)/shard_map/nxcf,xfd->nxcd/dot_general | solution.py:152
  277.6 17.9 %all-reduce.5.cloned.1.call-done = bf16[16,12,2048]{2,0,1:T(8,128)(2,1)} async-done(((bf16[16,12,2048]{2,0,1:T(8,128)(2,1)}), bf16[16,12,2048]{2,0,1:T(8,128)(2,1)}) %all-reduce.5.cloned.1.call-update) | async-done | bytes 786448 | tf_op jit(solution)/shard_map/psum | solution.py:155
  295.5 2.6 copy.65
  298.1 7.1 %all-to-all-start.2 = ((bf16[16,12,2048]{2,1,0:T(8,128)(2,1)}), bf16[16,12,2048]{2,1,0:T(8,128)(2,1)}, u32[]{:S(2)}, u32[]{:S(2)}) async-start(bf16[16,12,2048]{2,1,0:T(8,128)(2,1)} %copy.65), calls=%async_computation.3 | async-start | bytes 2097152 | tf_op jit(solution)/shard_map/all_to_all | solution.py:157
  305.2 0.1 reduce_sum.70
  305.4 0.7 copy.66
  306.0 25.1 %all-to-all-done.2 = bf16[16,12,2048]{2,1,0:T(8,128)(2,1)} async-done(((bf16[16,12,2048]{2,1,0:T(8,128)(2,1)}), bf16[16,12,2048]{2,1,0:T(8,128)(2,1)}, u32[]{:S(2)}, u32[]{:S(2)}) %all-to-all-start.2) | async-done | bytes 786464 | tf_op jit(solution)/shard_map/all_to_all | solution.py:157
  331.1 2.1 reshape.169
  333.2 1.5 fusion.18
  334.7 0.7 fusion.43
  (51 shorter events, 0.9 us)
Async XLA Ops:
  7.2 265.2 %copy-start = (bf16[1,704,2048]{2,1,0:T(8,128)(2,1)S(1)}, bf16[1,704,2048]{2,1,0:T(8,128)(2,1)}, u32[]{:S(2)}) copy-start(bf16[1,704,2048]{2,1,0:T(8,128)(2,1)} %param.39) | copy-start | bytes 8650756
  10.1 13.8 %all-to-all-start = ((bf16[32,16,128]{2,0,1:T(8,128)(2,1)}), bf16[32,16,128]{2,0,1:T(8,128)(2,1)S(1)}, u32[]{:S(2)}, u32[]{:S(2)}) async-start(bf16[32,16,128]{2,0,1:T(8,128)(2,1)} %copy_bitcast_fusion), calls=%async_computation | async-start | bytes 262144 | tf_op jit(solution)/shard_map/all_to_all | solution.py:82
  17.3 135.7 %reduce-scatter.2.cloned.1.call-start = ((), (), s32[]{:S(2)}) async-start(), calls=%async_computation.4 | async-start | bytes 2506752 | tf_op jit(solution)/shard_map/reduce_scatter | solution.py:84
  18.9 7.6 %copy-start.13 = (f32[32,4]{0,1:T(4,128)S(1)}, f32[32,4]{0,1:T(4,128)}, u32[]{:S(2)}) copy-start(f32[32,4]{0,1:T(4,128)} %param.35) | copy-start | bytes 1540
  18.9 7.7 %copy-start.7 = (s32[32,3]{0,1:T(4,128)S(1)}, s32[32,3]{0,1:T(4,128)}, u32[]{:S(2)}) copy-start(s32[32,3]{0,1:T(4,128)} %param.40) | copy-start | bytes 1156
  23.9 130.5 %copy-start.10 = (f32[4]{0:T(128)S(1)}, f32[4]{0:T(128)}, u32[]{:S(2)}) copy-start(f32[4]{0:T(128)} %param.30) | copy-start | bytes 52
  23.9 130.5 %copy-start.15 = (f32[4]{0:T(128)S(1)}, f32[4]{0:T(128)}, u32[]{:S(2)}) copy-start(f32[4]{0:T(128)} %param.29) | copy-start | bytes 52
  23.9 132.2 %copy-start.5 = (f32[32,4,64]{2,1,0:T(4,128)S(1)}, f32[32,4,64]{2,1,0:T(4,128)}, u32[]{:S(2)}) copy-start(f32[32,4,64]{2,1,0:T(4,128)} %param.34) | copy-start | bytes 98308
  25.8 179.9 %all-gather.2.cloned.1.call-start = ((), (), s32[]{:S(2)}) async-start(), calls=%async_computation.5 | async-start | bytes 1114112 | tf_op jit(solution)/shard_map/all_gather | solution.py:116
  26.5 200.0 %all-reduce.3.cloned.1.call-start = ((), (), s32[]{:S(2)}) async-start(), calls=%async_computation.6 | async-start | bytes 262144 | tf_op jit(solution)/shard_map/psum | solution.py:119
  27.3 180.6 %copy-start.11 = (s32[96]{0:T(128)}, s32[96]{0:T(128)S(1)}, u32[]{:S(2)}) copy-start(s32[96]{0:T(128)S(1)} %select_reduce_fusion) | copy-start | bytes 1156
  160.7 2.0 copy-start.1
  162.7 43.0 %copy-start.14 = (f32[256]{0:T(256)S(1)}, f32[256]{0:T(256)}, u32[]{:S(2)}) copy-start(f32[256]{0:T(256)} %param.31) | copy-start | bytes 3076
  162.7 63.8 %copy-start.2 = (bf16[32,2048]{1,0:T(8,128)(2,1)S(1)}, bf16[32,2048]{1,0:T(8,128)(2,1)}, u32[]{:S(2)}) copy-start(bf16[32,2048]{1,0:T(8,128)(2,1)} %param.21) | copy-start | bytes 393220
  162.7 64.9 %copy-start.6 = (f32[2048]{0:T(1024)S(1)}, f32[2048]{0:T(1024)}, u32[]{:S(2)}) copy-start(f32[2048]{0:T(1024)} %param.36) | copy-start | bytes 24580
  207.9 87.6 %all-reduce.5.cloned.1.call-start = ((), (), s32[]{:S(2)}) async-start(), calls=%async_computation.7 | async-start | bytes 1572864 | tf_op jit(solution)/shard_map/psum | solution.py:155
  267.5 1.0 copy-start.4
  277.5 27.7 %copy-start.12 = (s32[96]{0:T(128)S(1)}, s32[96]{0:T(128)}, u32[]{:S(2)}) copy-start(s32[96]{0:T(128)} %copy-done.11) | copy-start | bytes 1156
  277.5 27.8 %copy-start.8 = (s32[32,3]{0,1:T(4,128)S(1)}, s32[32,3]{0,1:T(4,128)}, u32[]{:S(2)}) copy-start(s32[32,3]{0,1:T(4,128)} %param.40) | copy-start | bytes 1156
  277.6 55.7 %copy-start.9 = (f32[32,3]{0,1:T(4,128)S(1)}, f32[32,3]{0,1:T(4,128)}, u32[]{:S(2)}) copy-start(f32[32,3]{0,1:T(4,128)} %param.41) | copy-start | bytes 1156
  298.1 36.6 %copy-start.3 = (bf16[32,2048]{1,0:T(8,128)(2,1)S(1)}, bf16[32,2048]{1,0:T(8,128)(2,1)}, u32[]{:S(2)}) copy-start(bf16[32,2048]{1,0:T(8,128)(2,1)} %all-reduce.3.cloned.1.call-done) | copy-start | bytes 393220
  298.1 33.0 %all-to-all-start.2 = ((bf16[16,12,2048]{2,1,0:T(8,128)(2,1)}), bf16[16,12,2048]{2,1,0:T(8,128)(2,1)}, u32[]{:S(2)}, u32[]{:S(2)}) async-start(bf16[16,12,2048]{2,1,0:T(8,128)(2,1)} %copy.65), calls=%async_computation.3 | async-start | bytes 2097152 | tf_op jit(solution)/shard_map/all_to_all | solution.py:157
Sparse Core Ops, SparseCore 0:
  25.9 127.0 reduce-scatter.1
  155.7 49.9 all-gather.1
  208.6 17.9 all-reduce.2
  277.7 17.7 all-reduce.4
where the time goes:
time: 343 us; the launch traced here: 342 us
  waiting for transfers between devices  230 us (67%)
  blocking collectives  33.1 us (10%)
  matrix products  20.2 us (6%)
  local copies, waits for them, and re-layouts  15.4 us (4%)
  starting transfers between devices  14.5 us (4%)
  other arithmetic  14.3 us (4%)
  between operations  14 us (4%)
    reduce_scatter x1, waiting for transfers between devices, body(): lax.psum_scatter(jnp.dot(spread, joined, preferred_element_type=jnp.float...  126 us
    all_gather x1, waiting for transfers between devices, body(): lax.all_gather(w_out, 'ep', axis=1, tiled=True)  39 us
    all_to_all x1, blocking collectives, body(): lax.all_to_all(outgoing, 'ep', split_axis=0, concat_axis=0, tiled=True)  33.1 us
    all_to_all x1, waiting for transfers between devices, body(): lax.all_to_all(finished, 'ep', split_axis=0, concat_axis=0, tiled=True)  25.1 us
    psum x1, waiting for transfers between devices, body(): lax.psum(partial_out.astype(jnp.bfloat16), 'tp').astype(jnp.float32)  18.1 us
    psum x1, waiting for transfers between devices, body(): expert_sum = lax.psum(partial_down.astype(jnp.bfloat16), 'tp')  17.9 us
    all_to_all x1, starting transfers between devices, body(): lax.all_to_all(normed, 'ep', split_axis=1, concat_axis=0, tiled=True)  7.22 us
    all_to_all x1, starting transfers between devices, body(): lax.all_to_all(finished, 'ep', split_axis=0, concat_axis=0, tiled=True)  7.11 us
  transfers between devices with their start and end apart: 6, of which 6 were waited for; matrix products, arithmetic and copies ran while one was open for 5% of the time, Pallas kernels for 0%

commit v1 on v0

--- a/solution.py
+++ b/solution.py
@@ -152,7 +152,9 @@
     partial_down = jnp.einsum(
         "nxcf,xfd->nxcd", hidden, w_expert_down, preferred_element_type=jnp.float32
     )
-    expert_sum = lax.psum(partial_down.astype(jnp.bfloat16), "tp")
+    x = partial_down.astype(jnp.bfloat16)
+    terms = lax.all_gather(x, "tp")
+    expert_sum = jnp.sum(terms, axis=0)
     finished = expert_sum.reshape(ep_count * local_experts, slot_count, width)
     returned = lax.all_to_all(finished, "ep", split_axis=0, concat_axis=0, tiled=True)
     picked = jnp.dot(

time: 343 us -> 337 us (0.983)
  waiting for transfers between devices: 230 us -> 221 us
    psum x1 -> x0, waiting for transfers between devices: 17.9 us -> none  [body(): expert_sum = lax.psum(partial_down.astype(jnp.bfloat16), 'tp')]
    all_gather x0 -> x1, waiting for transfers between devices: none -> 8.72 us  [body(): terms = lax.all_gather(x, 'tp')]
where the time goes in v1:
time: 337 us; the launch traced here: 336 us
  waiting for transfers between devices  221 us (66%)
  blocking collectives  33.1 us (10%)
  matrix products  20.2 us (6%)
  other arithmetic  17.1 us (5%)
  local copies, waits for them, and re-layouts  15.5 us (5%)
  starting transfers between devices  14.5 us (4%)
  between operations  14 us (4%)
    reduce_scatter x1, waiting for transfers between devices, body(): lax.psum_scatter(jnp.dot(spread, joined, preferred_element_type=jnp.float...  126 us
    all_gather x1, waiting for transfers between devices, body(): lax.all_gather(w_out, 'ep', axis=1, tiled=True)  39 us
    all_to_all x1, blocking collectives, body(): lax.all_to_all(outgoing, 'ep', split_axis=0, concat_axis=0, tiled=True)  33.1 us
    all_to_all x1, waiting for transfers between devices, body(): lax.all_to_all(finished, 'ep', split_axis=0, concat_axis=0, tiled=True)  25.1 us
    psum x1, waiting for transfers between devices, body(): lax.psum(partial_out.astype(jnp.bfloat16), 'tp').astype(jnp.float32)  18.1 us
    all_gather x1, waiting for transfers between devices, body(): terms = lax.all_gather(x, 'tp')  8.72 us
    all_to_all x1, starting transfers between devices, body(): lax.all_to_all(normed, 'ep', split_axis=1, concat_axis=0, tiled=True)  7.22 us
    all_to_all x1, starting transfers between devices, body(): lax.all_to_all(finished, 'ep', split_axis=0, concat_axis=0, tiled=True)  7.11 us
  transfers between devices with their start and end apart: 6, of which 6 were waited for; matrix products, arithmetic and copies ran while one was open for 5% of the time, Pallas kernels for 0%

profile of v1, /device:TPU:8, one launch (start us, length us, event | category | flops | bytes accessed | tf_op | source)
XLA Modules:
  0.0 335.7 jit_solution(10620202556017459230)
XLA Ops:
  7.2 1.2 fusion.37
  8.4 1.7 copy_bitcast_fusion
  10.1 7.2 %all-to-all-start = ((bf16[32,16,128]{2,0,1:T(8,128)(2,1)}), bf16[32,16,128]{2,0,1:T(8,128)(2,1)S(1)}, u32[]{:S(2)}, u32[]{:S(2)}) async-start(bf16[32,16,128]{2,0,1:T(8,128)(2,1)} %copy_bitcast_fusion), calls=%async_computation | async-start | bytes 262144 | tf_op jit(solution)/shard_map/all_to_all | solution.py:82
  17.3 0.8 copy.69
  18.1 0.8 copy.70
  19.0 1.1 concatenate.3
  20.0 3.9 %all-to-all-done = bf16[32,16,128]{2,0,1:T(8,128)(2,1)S(1)} async-done(((bf16[32,16,128]{2,0,1:T(8,128)(2,1)}), bf16[32,16,128]{2,0,1:T(8,128)(2,1)S(1)}, u32[]{:S(2)}, u32[]{:S(2)}) %all-to-all-start) | async-done | bytes 131104 | tf_op jit(solution)/shard_map/all_to_all | solution.py:82
  23.9 1.9 fusion.63
  25.8 0.7 all-gather.4.cloned.1.call-update
  26.8 0.1 eq.50
  27.0 0.1 reduce_window_sum.11
  27.1 0.2 select_reduce_fusion
  27.3 125.7 %reduce-scatter.2.cloned.1.call-done = f32[32,1032]{1,0:T(8,128)} async-done(((f32[512,1032]{1,0:T(8,128)}), f32[32,1032]{1,0:T(8,128)}) %reduce-scatter.2.cloned.1.call-update) | async-done | bytes 132112 | tf_op jit(solution)/shard_map/reduce_scatter | solution.py:84
  153.0 0.9 convert.10
  154.1 0.1 reshape.172
  154.4 0.9 broadcast_multiply_fusion.3
  155.3 0.8 subtract_exponential_fusion.1
  156.1 0.8 multiply_reduce_fusion.1
  156.9 3.8 %multiply_add_fusion = f32[32,4,64,64]{3,2,1,0:T(8,128)S(1)} fusion(f32[32,4,64,64]{3,2,1,0:T(8,128)} %param.33, f32[32,4,64]{2,1,0:T(4,128)S(1)} %get-tuple-element.34, f32[32,4,64]{2,1,0:T(4,128)S(1)} %get-tuple-element.35, f32[32,4]{1,0:T(8,128)S(1)} %subtract_exponential_fusion.1), kind=kLoop, calls=%fused_computation | loop fusion | flops 1572864 | bytes 4260352 | tf_op jit(solution)/shard_map/add | solution.py:38
  160.7 2.0 copy-done.1
  162.7 3.4 fusion.64
  166.1 0.2 fusion.60
  166.3 0.2 multiply_reduce_fusion
  166.5 0.1 subtract_multiply_fusion
  166.6 0.1 reshape.152
  166.7 39.0 %all-gather.4.cloned.1.call-done = bf16[256,2048]{1,0:T(8,128)(2,1)} async-done(((bf16[256,128]{1,0:T(8,128)(2,1)}), bf16[256,2048]{1,0:T(8,128)(2,1)}) %all-gather.4.cloned.1.call-update) | async-done | bytes 1048592 | tf_op jit(solution)/shard_map/all_gather | solution.py:116
  205.7 2.2 convolution_convert_fusion.1
  207.9 0.5 multiply_add_fusion.3
  208.4 18.1 %all-reduce.2.cloned.1.call-done = bf16[32,2048]{1,0:T(8,128)(2,1)} async-done(((bf16[32,2048]{1,0:T(8,128)(2,1)}), bf16[32,2048]{1,0:T(8,128)(2,1)}) %all-reduce.2.cloned.1.call-update) | async-done | bytes 131088 | tf_op jit(solution)/shard_map/psum | solution.py:119
  226.5 1.1 fusion.41
  227.6 1.0 fusion.43
  228.6 0.2 broadcast_in_dim.2
  228.8 1.1 reshape.153
  229.9 2.4 convolution_convert_fusion
  232.3 2.2 reshape.154
  234.5 33.1 %all_to_all.29 = bf16[16,12,2048]{2,1,0:T(8,128)(2,1)S(1)} all-to-all(bf16[16,12,2048]{2,1,0:T(8,128)(2,1)} %reshape.154), channel_id=1, replica_groups=mesh['ep'=16,'tp'=2] {'ep'}, dimensions={0} | all-to-all | bytes 1572864 | tf_op jit(solution)/shard_map/all_to_all | solution.py:142
  267.6 1.0 copy-done.4
  268.6 3.8 %fusion.12 = f32[16,1,12,704]{3,0,2,1:T(8,128)} fusion(bf16[1,2048,704]{1,2,0:T(8,128)(2,1)} %param.37, bf16[16,12,2048]{2,1,0:T(8,128)(2,1)S(1)} %all_to_all.29), kind=kOutput, calls=%fused_computation.12 | convolution fusion | flops 553648128 | bytes 4210688 | tf_op jit(solution)/shard_map/nxcd,xdf->nxcf/dot_general | solution.py:145
  272.4 5.2 %fusion.9 = bf16[16,1,12,2048]{3,0,2,1:T(8,128)(2,1)} fusion(bf16[1,704,2048]{2,1,0:T(8,128)(2,1)S(1)} %copy-done, bf16[1,2048,704]{1,2,0:T(8,128)(2,1)} %param.38, f32[16,1,12,704]{3,0,2,1:T(8,128)} %fusion.12, bf16[16,12,2048]{2,1,0:T(8,128)(2,1)} %copy-done.4), kind=kOutput, calls=%fused_computation.9 | convolution fusion | flops 1108500480 | bytes 7880704 | tf_op jit(solution)/shard_map/nxcf,xfd->nxcd/dot_general | solution.py:152
  277.6 8.7 %all-gather.6.cloned.1.call-done = bf16[32,1,12,2048]{3,0,2,1:T(8,128)(2,1)} async-done(((bf16[16,1,12,2048]{3,0,2,1:T(8,128)(2,1)}), bf16[32,1,12,2048]{3,0,2,1:T(8,128)(2,1)}) %all-gather.6.cloned.1.call-update) | async-done | bytes 1572880 | tf_op jit(solution)/shard_map/all_gather | solution.py:156
  286.3 2.8 reduce.2
  289.2 2.6 copy.76
  291.8 7.1 %all-to-all-start.2 = ((bf16[16,12,2048]{2,1,0:T(8,128)(2,1)}), bf16[16,12,2048]{2,1,0:T(8,128)(2,1)}, u32[]{:S(2)}, u32[]{:S(2)}) async-start(bf16[16,12,2048]{2,1,0:T(8,128)(2,1)} %copy.76), calls=%async_computation.3 | async-start | bytes 2097152 | tf_op jit(solution)/shard_map/all_to_all | solution.py:159
  299.1 0.7 copy.77
  299.7 25.1 %all-to-all-done.2 = bf16[16,12,2048]{2,1,0:T(8,128)(2,1)} async-done(((bf16[16,12,2048]{2,1,0:T(8,128)(2,1)}), bf16[16,12,2048]{2,1,0:T(8,128)(2,1)}, u32[]{:S(2)}, u32[]{:S(2)}) %all-to-all-start.2) | async-done | bytes 786464 | tf_op jit(solution)/shard_map/all_to_all | solution.py:159
  324.9 2.1 reshape.170
  327.0 1.5 fusion.21
  328.5 0.7 fusion.44
  (52 shorter events, 1.0 us)
Async XLA Ops:
  7.2 265.2 %copy-start = (bf16[1,704,2048]{2,1,0:T(8,128)(2,1)S(1)}, bf16[1,704,2048]{2,1,0:T(8,128)(2,1)}, u32[]{:S(2)}) copy-start(bf16[1,704,2048]{2,1,0:T(8,128)(2,1)} %param.39) | copy-start | bytes 8650756
  10.1 13.8 %all-to-all-start = ((bf16[32,16,128]{2,0,1:T(8,128)(2,1)}), bf16[32,16,128]{2,0,1:T(8,128)(2,1)S(1)}, u32[]{:S(2)}, u32[]{:S(2)}) async-start(bf16[32,16,128]{2,0,1:T(8,128)(2,1)} %copy_bitcast_fusion), calls=%async_computation | async-start | bytes 262144 | tf_op jit(solution)/shard_map/all_to_all | solution.py:82
  17.3 135.7 %reduce-scatter.2.cloned.1.call-start = ((), (), s32[]{:S(2)}) async-start(), calls=%async_computation.4 | async-start | bytes 2506752 | tf_op jit(solution)/shard_map/reduce_scatter | solution.py:84
  18.9 7.6 %copy-start.13 = (f32[32,4]{0,1:T(4,128)S(1)}, f32[32,4]{0,1:T(4,128)}, u32[]{:S(2)}) copy-start(f32[32,4]{0,1:T(4,128)} %param.35) | copy-start | bytes 1540
  18.9 7.7 %copy-start.7 = (s32[32,3]{0,1:T(4,128)S(1)}, s32[32,3]{0,1:T(4,128)}, u32[]{:S(2)}) copy-start(s32[32,3]{0,1:T(4,128)} %param.40) | copy-start | bytes 1156
  23.9 130.5 %copy-start.10 = (f32[4]{0:T(128)S(1)}, f32[4]{0:T(128)}, u32[]{:S(2)}) copy-start(f32[4]{0:T(128)} %param.30) | copy-start | bytes 52
  23.9 130.5 %copy-start.15 = (f32[4]{0:T(128)S(1)}, f32[4]{0:T(128)}, u32[]{:S(2)}) copy-start(f32[4]{0:T(128)} %param.29) | copy-start | bytes 52
  23.9 132.2 %copy-start.5 = (f32[32,4,64]{2,1,0:T(4,128)S(1)}, f32[32,4,64]{2,1,0:T(4,128)}, u32[]{:S(2)}) copy-start(f32[32,4,64]{2,1,0:T(4,128)} %param.34) | copy-start | bytes 98308
  25.8 179.9 %all-gather.4.cloned.1.call-start = ((), (), s32[]{:S(2)}) async-start(), calls=%async_computation.5 | async-start | bytes 1114112 | tf_op jit(solution)/shard_map/all_gather | solution.py:116
  26.5 200.0 %all-reduce.2.cloned.1.call-start = ((), (), s32[]{:S(2)}) async-start(), calls=%async_computation.6 | async-start | bytes 262144 | tf_op jit(solution)/shard_map/psum | solution.py:119
  27.3 180.6 %copy-start.11 = (s32[96]{0:T(128)}, s32[96]{0:T(128)S(1)}, u32[]{:S(2)}) copy-start(s32[96]{0:T(128)S(1)} %select_reduce_fusion) | copy-start | bytes 1156
  160.7 2.0 copy-start.1
  162.7 43.0 %copy-start.14 = (f32[256]{0:T(256)S(1)}, f32[256]{0:T(256)}, u32[]{:S(2)}) copy-start(f32[256]{0:T(256)} %param.31) | copy-start | bytes 3076
  162.7 63.8 %copy-start.2 = (bf16[32,2048]{1,0:T(8,128)(2,1)S(1)}, bf16[32,2048]{1,0:T(8,128)(2,1)}, u32[]{:S(2)}) copy-start(bf16[32,2048]{1,0:T(8,128)(2,1)} %param.21) | copy-start | bytes 393220
  162.7 64.9 %copy-start.6 = (f32[2048]{0:T(1024)S(1)}, f32[2048]{0:T(1024)}, u32[]{:S(2)}) copy-start(f32[2048]{0:T(1024)} %param.36) | copy-start | bytes 24580
  207.9 78.4 %all-gather.6.cloned.1.call-start = ((), (), s32[]{:S(2)}) async-start(), calls=%async_computation.7 | async-start | bytes 2359296 | tf_op jit(solution)/shard_map/all_gather | solution.py:156
  267.6 1.0 copy-start.4
  286.3 12.6 %copy-start.12 = (s32[96]{0:T(128)S(1)}, s32[96]{0:T(128)}, u32[]{:S(2)}) copy-start(s32[96]{0:T(128)} %copy-done.11) | copy-start | bytes 1156
  286.3 12.8 %copy-start.8 = (s32[32,3]{0,1:T(4,128)S(1)}, s32[32,3]{0,1:T(4,128)}, u32[]{:S(2)}) copy-start(s32[32,3]{0,1:T(4,128)} %param.40) | copy-start | bytes 1156
  289.2 37.8 %copy-start.9 = (f32[32,3]{0,1:T(4,128)S(1)}, f32[32,3]{0,1:T(4,128)}, u32[]{:S(2)}) copy-start(f32[32,3]{0,1:T(4,128)} %param.41) | copy-start | bytes 1156
  291.8 36.7 %copy-start.3 = (bf16[32,2048]{1,0:T(8,128)(2,1)S(1)}, bf16[32,2048]{1,0:T(8,128)(2,1)}, u32[]{:S(2)}) copy-start(bf16[32,2048]{1,0:T(8,128)(2,1)} %all-reduce.2.cloned.1.call-done) | copy-start | bytes 393220
  291.8 33.1 %all-to-all-start.2 = ((bf16[16,12,2048]{2,1,0:T(8,128)(2,1)}), bf16[16,12,2048]{2,1,0:T(8,128)(2,1)}, u32[]{:S(2)}, u32[]{:S(2)}) async-start(bf16[16,12,2048]{2,1,0:T(8,128)(2,1)} %copy.76), calls=%async_computation.3 | async-start | bytes 2097152 | tf_op jit(solution)/shard_map/all_to_all | solution.py:159
Sparse Core Ops, SparseCore 0:
  25.9 127.0 reduce-scatter.1
  155.7 49.9 all-gather.3
  208.6 17.9 all-reduce.1
  277.7 8.5 all-gather.5
